TPU v7x, 32 devices: a whole 2x2x4 slice. The times are simulated.
32 devices in a mesh: gr: 2 (over x), sp: 8 (over z, y), tp: 2 (over core).
Axes of the slice: x: 2, y: 2, z: 4, core: 2. Of those that a mesh axis runs over, the one named last changes fastest.
Arguments:
- prompt_block_input: bfloat16 [16, 2048, 2048], P('gr', 'sp'), may hold values from -6 to 6
- key_projection_weight: bfloat16 [2048, 512], P(None, 'tp'), may hold values from -0.125 to 0.125
- value_projection_weight: bfloat16 [2048, 512], P(None, 'tp'), may hold values from -0.125 to 0.125
- forget_gate_weight: bfloat16 [8, 2048], P('tp'), may hold values from -0.125 to 0.125
- forget_gate_bias: float32 [8], P('tp'), may hold values from 3.5 to 12
- forget_gate_scale: float32 [16, 8, 2048], P('gr', 'tp', 'sp'), may hold values from 0.15 to 6
- gate_spike_added: float32 [16, 8, 2048], P('gr', 'tp', 'sp'), may hold values from -0.7 to 0
- prior_key_value_cache: bfloat16 [16, 14336, 8, 128], P(('gr', 'sp'), None, 'tp')
- prior_cumulative_log_forget: float32 [16, 8, 14336], P(('gr', 'sp'), 'tp'), as said below
- decoded_token_query: bfloat16 [16, 1024], P('gr', 'tp')
- decoded_token_key: bfloat16 [16, 512], P(('gr', 'sp'), 'tp'), may hold values from -6 to 6
- decoded_token_value: bfloat16 [16, 512], P(('gr', 'sp'), 'tp'), may hold values from -6 to 6
- decoded_log_gate: float32 [16, 8], P(('gr', 'sp'), 'tp'), may hold values from -2.5 to -0.05
- key_norm_gain: float32 [64], replicated, may hold values from 0.1 to 1.9
- read_norm_gain: float32 [1024], P('tp'), may hold values from 0.1 to 1.9
Outputs:
- new_cache: bfloat16 [16, 2048, 8, 128], P(('gr', 'sp'), None, 'tp')
- new_logc: float32 [16, 8, 2048], P(('gr', 'sp'), 'tp')
- next_read: bfloat16 [16, 1024], P(('gr', 'sp'), 'tp')
Inputs may be any that keep to these rules, and one draw needn't show every extreme that they name: `prior_cumulative_log_forget`: each position's cumulative log forget value from the start of its sequence.
All inputs are finite; a program needn't handle non-finite values.
Results may differ from a plain program's by a relative error of at most 0.008.
Values may be sent and summed in bfloat16 or wider, within the bound.
A program may use at most 128 MiB of HBM per device.

v0:
```python
import jax
import jax.numpy as jnp
from jax import lax
from jax.sharding import PartitionSpec as P

EPSILON = 1e-06


def project(
    tok_rows,
    key_projection_weight,
    value_projection_weight,
    forget_gate_weight,
    forget_gate_bias,
    key_norm_gain,
):
    head_dim = key_norm_gain.shape[0]
    key_raw = jnp.einsum(
        "spd,dc->spc", tok_rows, key_projection_weight, preferred_element_type=jnp.float32
    )
    split_heads = key_raw.reshape(key_raw.shape[:2] + (-1, head_dim))
    normed = (
        split_heads
        * lax.rsqrt(jnp.mean(split_heads * split_heads, axis=-1, keepdims=True) + EPSILON)
        * key_norm_gain
    )
    block_keys = normed.astype(jnp.bfloat16)
    block_values = jnp.einsum(
        "spd,dc->spc", tok_rows, value_projection_weight, preferred_element_type=jnp.float32
    )
    block_values = block_values.reshape(split_heads.shape).astype(jnp.bfloat16)
    cache_rows = jnp.concatenate([block_keys, block_values], axis=-1)
    gate_preactivation = jnp.einsum(
        "spd,hd->shp", tok_rows, forget_gate_weight, preferred_element_type=jnp.float32
    )
    return (cache_rows, gate_preactivation + forget_gate_bias[None, :, None])


def forget_value_rows(gate_preactivation, forget_gate_scale, gate_spike_added):
    return forget_gate_scale * jax.nn.log_sigmoid(gate_preactivation) + gate_spike_added


def query_split(query, kv_count, head_dim):
    return query.reshape(query.shape[0], kv_count, -1, head_dim)


def head_scores(query, cache_rows, head_dim):
    query_heads = query_split(query, cache_rows.shape[2], head_dim)
    key_heads = cache_rows[..., :head_dim]
    return jnp.einsum(
        "skge,slke->skgl", query_heads, key_heads, preferred_element_type=jnp.float32
    ) * head_dim ** (-0.5)


def weigh(scores, cache_rows, head_dim):
    row_top = jnp.max(scores, axis=-1)
    weights = jnp.exp(scores - row_top[..., None]).astype(jnp.bfloat16)
    value_heads = cache_rows[..., head_dim:]
    return (
        row_top,
        jnp.einsum("skgl,slke->skge", weights, value_heads, preferred_element_type=jnp.float32),
    )


def local(
    prompt_block_input,
    key_projection_weight,
    value_projection_weight,
    forget_gate_weight,
    forget_gate_bias,
    forget_gate_scale,
    gate_spike_added,
    prior_key_value_cache,
    prior_cumulative_log_forget,
    decoded_token_query,
    decoded_token_key,
    decoded_token_value,
    decoded_log_gate,
    key_norm_gain,
    read_norm_gain,
):
    head_dim = key_norm_gain.shape[0]
    own_count = prior_key_value_cache.shape[0]
    kv_count = prior_key_value_cache.shape[2]
    seq_start = lax.axis_index("sp") * own_count
    query_own = lax.dynamic_slice_in_dim(decoded_token_query, seq_start, own_count, 0)
    rows_local, gate_preactivation = project(
        prompt_block_input,
        key_projection_weight,
        value_projection_weight,
        forget_gate_weight,
        forget_gate_bias,
        key_norm_gain,
    )
    local_forget_values = forget_value_rows(gate_preactivation, forget_gate_scale, gate_spike_added)
    new_cache = lax.all_to_all(rows_local, "sp", split_axis=0, concat_axis=1, tiled=True)
    log_forget_value = lax.all_to_all(
        local_forget_values, "sp", split_axis=0, concat_axis=2, tiled=True
    )
    new_logc = prior_cumulative_log_forget[:, :, -1:] + jnp.cumsum(log_forget_value, axis=-1)
    final_logc = new_logc[:, :, -1] + decoded_log_gate
    past_scores = (
        head_scores(query_own, prior_key_value_cache, head_dim)
        + final_logc[:, :, None, None]
        - prior_cumulative_log_forget[:, :, None, :]
    )
    past_top, past_sum = weigh(past_scores, prior_key_value_cache, head_dim)
    block_scores = (
        head_scores(query_own, new_cache, head_dim)
        + final_logc[:, :, None, None]
        - new_logc[:, :, None, :]
    )
    block_top, block_sum = weigh(block_scores, new_cache, head_dim)
    query_heads = query_split(query_own, kv_count, head_dim)
    own_keys = decoded_token_key.reshape(own_count, kv_count, head_dim)
    own_score = jnp.einsum(
        "skge,ske->skg", query_heads, own_keys, preferred_element_type=jnp.float32
    ) * head_dim ** (-0.5)
    row_top = jnp.maximum(jnp.maximum(past_top, block_top), own_score)
    own_weight = jnp.exp(own_score - row_top).astype(jnp.bfloat16)
    weighted = (
        past_sum * jnp.exp(past_top - row_top)[..., None]
        + block_sum * jnp.exp(block_top - row_top)[..., None]
    )
    own_values = decoded_token_value.reshape(own_count, kv_count, 1, head_dim).astype(jnp.float32)
    weighted = weighted + own_weight.astype(jnp.float32)[..., None] * own_values
    normed = weighted * lax.rsqrt(jnp.mean(weighted * weighted, axis=-1, keepdims=True) + EPSILON)
    next_read = (normed.reshape(own_count, -1) * read_norm_gain).astype(jnp.bfloat16)
    return (new_cache, new_logc, next_read)


def solution(mesh):
    return jax.shard_map(
        local,
        mesh=mesh,
        in_specs=(
            P("gr", "sp", None),
            P(None, "tp"),
            P(None, "tp"),
            P("tp", None),
            P("tp"),
            P("gr", "tp", "sp"),
            P("gr", "tp", "sp"),
            P(("gr", "sp"), None, "tp", None),
            P(("gr", "sp"), "tp", None),
            P("gr", "tp"),
            P(("gr", "sp"), "tp"),
            P(("gr", "sp"), "tp"),
            P(("gr", "sp"), "tp"),
            P(),
            P("tp"),
        ),
        out_specs=(
            P(("gr", "sp"), None, "tp", None),
            P(("gr", "sp"), "tp", None),
            P(("gr", "sp"), "tp"),
        ),
        check_vma=False,
    )
```

profile of v0, /device:TPU:0, one launch (start us, length us, event | category | flops | bytes accessed | tf_op | source)
XLA Modules:
  0.0 118.0 jit_solution(34637716511074179)
XLA Ops:
  0.6 6.4 %fusion.20 = f32[8,4,256]{2,1,0:T(4,128)} fusion(f32[8,4,256]{2,1,0:T(4,128)} %param.21, f32[8,4,256]{2,1,0:T(4,128)} %param.20, bf16[8,256,2048]{2,1,0:T(8,128)(2,1)} %param.15, bf16[4,2048]{1,0:T(4,128)(2,1)} %param.18, f32[4]{0:T(128)} %param.19), kind=kOutput, calls=%fused_computation.31 | convolution fusion | flops 33644544 | bytes 8503312 | tf_op jit(solution)/shard_map/spd,hd->shp/dot_general | solution.py:33
  7.0 7.3 %all-to-all-start.1 = ((f32[8,4,256]{2,1,0:T(4,128)}), f32[8,4,256]{2,1,0:T(4,128)S(1)}, u32[]{:S(2)}, u32[]{:S(2)}) async-start(f32[8,4,256]{2,1,0:T(4,128)} %fusion.20), calls=%async_computation.1 | async-start | bytes 65536 | tf_op jit(solution)/shard_map/all_to_all | solution.py:97
  14.4 5.9 %multiply_reduce_fusion = (f32[8,256,4]{1,2,0:T(4,128)S(1)}, f32[8,256,256]{1,2,0:T(8,128)S(1)}) fusion(bf16[8,256,2048]{2,1,0:T(8,128)(2,1)} %param.15, bf16[2048,256]{1,0:T(8,128)(2,1)S(1)} %copy-done), kind=kOutput, calls=%fused_computation.11 | convolution fusion | flops 2148524032 | bytes 11567104 | tf_op jit(solution)/shard_map/spd,dc->spc/dot_general | solution.py:18
  20.4 2.4 %convolution_convert_fusion = bf16[8,256,256]{1,2,0:T(8,128)(2,1)S(1)} fusion(bf16[8,256,2048]{2,1,0:T(8,128)(2,1)S(1)} %copy-done.2, bf16[2048,256]{1,0:T(8,128)(2,1)S(1)} %copy-done.9), kind=kOutput, calls=%fused_computation.12 | convolution fusion | flops 2148007936 | bytes 10485760 | tf_op jit(solution)/shard_map/spd,dc->spc/dot_general | solution.py:28
  22.8 0.6 multiply_convert_fusion
  23.4 1.5 %pad_maximum_fusion = bf16[8,256,4,128]{1,3,2,0:T(8,128)(2,1)} fusion(bf16[8,256,4,64]{1,3,2,0:T(8,128)(2,1)S(1)} %bitcast.80, bf16[8,256,4,64]{1,3,2,0:T(8,128)(2,1)S(1)} %multiply_convert_fusion), kind=kLoop, calls=%fused_computation.9 | loop fusion | flops 4194304 | bytes 4194304 | tf_op jit(solution)/shard_map/concatenate | solution.py:32
  24.9 6.0 %all-to-all-start = ((bf16[8,256,4,128]{1,3,2,0:T(8,128)(2,1)}), bf16[8,256,4,128]{1,3,2,0:T(8,128)(2,1)S(1)}, u32[]{:S(2)}, u32[]{:S(2)}) async-start(bf16[8,256,4,128]{1,3,2,0:T(8,128)(2,1)} %pad_maximum_fusion), calls=%async_computation | async-start | bytes 4194304 | tf_op jit(solution)/shard_map/all_to_all | solution.py:96
  30.8 20.9 %fusion.26 = (bf16[1,14336,4,64]{3,2,1,0:T(4,128)(2,1)}, bf16[1,14336,4,64]{3,2,1,0:T(4,128)(2,1)}) fusion(bf16[1,14336,4,128]{3,2,1,0:T(4,128)(2,1)} %param.22), kind=kLoop, calls=%fused_computation.56 | loop fusion | bytes 29360128 | tf_op jit(solution)/shard_map/slice | solution.py:49
  51.8 0.7 dynamic-slice_reduce_fusion
  52.6 21.4 %copy.37 = bf16[1,14336,4,64]{1,3,2,0:T(8,128)(2,1)} copy(bf16[1,14336,4,64]{3,2,1,0:T(4,128)(2,1)} %get-tuple-element.9) | data formatting | bytes 14680064
  74.1 21.4 %copy.38 = bf16[1,14336,4,64]{1,3,2,0:T(8,128)(2,1)} copy(bf16[1,14336,4,64]{3,2,1,0:T(4,128)(2,1)} %get-tuple-element.10) | data formatting | bytes 14680064
  95.7 0.2 slice_reduce_fusion.2
  96.0 1.2 reduce-window.6
  97.2 0.2 slice_reduce_fusion
  97.4 0.2 reduce-window.9
  97.7 0.2 slice_reduce_fusion.1
  98.1 4.9 %fusion.27 = (f32[4,2]{1,0:T(4,128)S(1)}, f32[4,2,14336]{2,1,0:T(2,128)}) fusion(f32[4,14336]{1,0:T(4,128)S(1)} %bitcast.79, f32[4]{0:T(128)S(1)} %fusion.25, bf16[4,2,64]{2,1,0:T(2,128)(2,1)S(1)} %reshape.260, bf16[1,14336,4,64]{1,3,2,0:T(8,128)(2,1)} %copy.37), kind=kOutput, calls=%fused_computation.57 | convolution fusion | flops 15138808 | bytes 8029232 | tf_op jit(solution)/shard_map/skge,slke->skgl/dot_general | solution.py:50
  103.0 2.5 %copy.26 = bf16[8,256,4,128]{1,0,3,2:T(8,128)(2,1)} copy(bf16[8,256,4,128]{1,3,2,0:T(8,128)(2,1)S(1)} %all-to-all-done) | data formatting | bytes 4194304 | tf_op jit(solution)/shard_map/all_to_all | solution.py:96
  105.5 3.0 %all_to_all.21 = bf16[1,2048,4,128]{1,3,2,0:T(8,128)(2,1)S(1)} reshape(bf16[8,256,4,128]{1,0,3,2:T(8,128)(2,1)} %copy.26) | data formatting | bytes 4194304 | tf_op jit(solution)/shard_map/all_to_all | solution.py:96
  108.5 2.5 %copy.30 = bf16[1,2048,4,128]{3,2,1,0:T(4,128)(2,1)} copy(bf16[1,2048,4,128]{1,3,2,0:T(8,128)(2,1)S(1)} %all_to_all.21) | data formatting | bytes 4194304
  111.1 0.3 fusion.28
  111.4 5.3 %fusion.11 = f32[4,2,64]{2,1,0:T(2,128)S(1)} fusion(bf16[1,14336,4,64]{1,3,2,0:T(8,128)(2,1)} %copy.38, f32[4,2,14336]{2,1,0:T(2,128)} %get-tuple-element.17, f32[4,2]{1,0:T(4,128)S(1)} %get-tuple-element.16, f32[4,2]{1,0:T(4,128)S(1)} %get-tuple-element.13), kind=kOutput, calls=%fused_computation.19 | convolution fusion | flops 14909952 | bytes 7800896 | tf_op jit(solution)/shard_map/skgl,slke->skge/dot_general | solution.py:61
  116.7 0.5 multiply_reduce_fusion.1
  117.4 0.6 convert_element_type.52
  (46 shorter events, 1.0 us)
Async XLA Ops:
  0.6 13.7 %copy-start = (bf16[2048,256]{1,0:T(8,128)(2,1)S(1)}, bf16[2048,256]{1,0:T(8,128)(2,1)}, u32[]{:S(2)}) copy-start(bf16[2048,256]{1,0:T(8,128)(2,1)} %param.16) | copy-start | bytes 3145732
  7.0 17.8 %all-to-all-start.1 = ((f32[8,4,256]{2,1,0:T(4,128)}), f32[8,4,256]{2,1,0:T(4,128)S(1)}, u32[]{:S(2)}, u32[]{:S(2)}) async-start(f32[8,4,256]{2,1,0:T(4,128)} %fusion.20), calls=%async_computation.1 | async-start | bytes 65536 | tf_op jit(solution)/shard_map/all_to_all | solution.py:97
  14.3 6.0 %copy-start.2 = (bf16[8,256,2048]{2,1,0:T(8,128)(2,1)S(1)}, bf16[8,256,2048]{2,1,0:T(8,128)(2,1)}, u32[]{:S(2)}) copy-start(bf16[8,256,2048]{2,1,0:T(8,128)(2,1)} %param.15) | copy-start | bytes 25165828
  14.4 6.0 %copy-start.9 = (bf16[2048,256]{1,0:T(8,128)(2,1)S(1)}, bf16[2048,256]{1,0:T(8,128)(2,1)}, u32[]{:S(2)}) copy-start(bf16[2048,256]{1,0:T(8,128)(2,1)} %param.17) | copy-start | bytes 3145732
  20.4 2.4 %copy-start.8 = (f32[64]{0:T(128)S(1)}, f32[64]{0:T(128)}, u32[]{:S(2)}) copy-start(f32[64]{0:T(128)} %param.28) | copy-start | bytes 772
  24.9 78.2 %all-to-all-start = ((bf16[8,256,4,128]{1,3,2,0:T(8,128)(2,1)}), bf16[8,256,4,128]{1,3,2,0:T(8,128)(2,1)S(1)}, u32[]{:S(2)}, u32[]{:S(2)}) async-start(bf16[8,256,4,128]{1,3,2,0:T(8,128)(2,1)} %pad_maximum_fusion), calls=%async_computation | async-start | bytes 4194304 | tf_op jit(solution)/shard_map/all_to_all | solution.py:96
  52.6 21.4 %copy-start.6 = (bf16[1,256]{1,0:T(2,128)(2,1)S(1)}, bf16[1,256]{1,0:T(2,128)(2,1)}, u32[]{:S(2)}) copy-start(bf16[1,256]{1,0:T(2,128)(2,1)} %param.25) | copy-start | bytes 1540
  74.1 21.5 %copy-start.7 = (bf16[1,256]{1,0:T(2,128)(2,1)S(1)}, bf16[1,256]{1,0:T(2,128)(2,1)}, u32[]{:S(2)}) copy-start(bf16[1,256]{1,0:T(2,128)(2,1)} %param.26) | copy-start | bytes 1540
  74.1 21.6 %copy-start.3 = (f32[1,4,14336]{2,1,0:T(4,128)S(1)}, f32[1,4,14336]{2,1,0:T(4,128)}, u32[]{:S(2)}) copy-start(f32[1,4,14336]{2,1,0:T(4,128)} %param.23) | copy-start | bytes 688132
  74.1 23.8 %copy-start.10 = (f32[1,4]{1,0:T(1,128)S(1)}, f32[1,4]{1,0:T(1,128)}, u32[]{:S(2)}) copy-start(f32[1,4]{1,0:T(1,128)} %param.27) | copy-start | bytes 52
  97.7 10.8 %copy-start.4 = (f32[1,4,2048]{2,1,0:T(4,128)}, f32[1,4,2048]{2,1,0:T(4,128)S(1)}, u32[]{:S(2)}) copy-start(f32[1,4,2048]{2,1,0:T(4,128)S(1)} %add_add_fusion) | copy-start | bytes 98308
  105.5 12.5 %copy-start.1 = (bf16[2048,256]{1,0:T(8,128)(2,1)S(1)}, bf16[2048,256]{1,0:T(8,128)(2,1)}, u32[]{:S(2)}) copy-start(bf16[2048,256]{1,0:T(8,128)(2,1)} %param.16) | copy-start | bytes 3145732
  108.5 8.9 %copy-start.5 = (f32[512]{0:T(512)S(1)}, f32[512]{0:T(512)}, u32[]{:S(2)}) copy-start(f32[512]{0:T(512)} %param.29) | copy-start | bytes 6148
where the time goes:
time: 119 us; the launch traced here: 118 us
  local copies, waits for them, and re-layouts  74.3 us (62%)
  matrix products  25.9 us (22%)
  starting transfers between devices  13.3 us (11%)
  other arithmetic  3.72 us (3%)
    unnamed x26, local copies, waits for them, and re-layouts  45.6 us
    slice x1, local copies, waits for them, and re-layouts, head_scores(): key_heads = cache_rows[..., :head_dim]  20.9 us
    all_to_all x1, starting transfers between devices, local(): lax.all_to_all(local_forget_values, 'sp', split_axis=0, concat_axis=2, ti...  7.31 us
    dot_general x1, matrix products, project(): jnp.einsum('spd,hd->shp', tok_rows, forget_gate_weight, preferred_element...  6.38 us
    all_to_all x1, starting transfers between devices, local(): lax.all_to_all(rows_local, 'sp', split_axis=0, concat_axis=1, tiled=True)  5.99 us
    dot_general x1, matrix products, project(): jnp.einsum('spd,dc->spc', tok_rows, key_projection_weight, preferred_elem...  5.92 us
    dot_general x2, matrix products, weigh(): jnp.einsum('skgl,slke->skge', weights, value_heads, preferred_element_typ...  5.84 us
    all_to_all x2, local copies, waits for them, and re-layouts, local(): lax.all_to_all(rows_local, 'sp', split_axis=0, concat_axis=1, tiled=True)  5.47 us
  transfers between devices with their start and end apart: 2, of which 0 were waited for; matrix products, arithmetic and copies ran while one was open for 70% of the time, Pallas kernels for 0%

commit v1 on v0

--- a/solution.py
+++ b/solution.py
@@ -94,9 +94,10 @@
     )
     local_forget_values = forget_value_rows(gate_preactivation, forget_gate_scale, gate_spike_added)
     new_cache = lax.all_to_all(rows_local, "sp", split_axis=0, concat_axis=1, tiled=True)
-    log_forget_value = lax.all_to_all(
-        local_forget_values, "sp", split_axis=0, concat_axis=2, tiled=True
+    _shape_vectors = lambda m: jnp.concatenate(
+        lax.all_to_all(jnp.stack(jnp.split(m, lax.axis_size("sp"), axis=0), 0), "sp", 0, 0), axis=2
     )
+    log_forget_value = _shape_vectors(local_forget_values)
     new_logc = prior_cumulative_log_forget[:, :, -1:] + jnp.cumsum(log_forget_value, axis=-1)
     final_logc = new_logc[:, :, -1] + decoded_log_gate
     past_scores = (

time: 119 us -> 124 us (1.042)
  local copies, waits for them, and re-layouts: 74.3 us -> 79 us
    unnamed x26 -> x33, local copies, waits for them, and re-layouts: 45.6 us -> 49.7 us
  transfers between devices with their start and end apart: 2 -> 2, of which waited for: 0 -> 0; matrix products, arithmetic and copies ran while one was open for 70% -> 68% of each run, Pallas kernels for 0% -> 0%
where the time goes in v1:
time: 124 us; the launch traced here: 122 us
  local copies, waits for them, and re-layouts  79 us (64%)
  matrix products  25.3 us (20%)
  starting transfers between devices  13.3 us (11%)
  other arithmetic  3.72 us (3%)
    unnamed x33, local copies, waits for them, and re-layouts  49.7 us
    slice x1, local copies, waits for them, and re-layouts, head_scores(): key_heads = cache_rows[..., :head_dim]  20.9 us
    all_to_all x1, starting transfers between devices, local(): lax.all_to_all(jnp.stack(jnp.split(m, lax.axis_size('sp'), axis=0), 0), '...  7.31 us
    all_to_all x1, starting transfers between devices, local(): lax.all_to_all(rows_local, 'sp', split_axis=0, concat_axis=1, tiled=True)  5.97 us
    dot_general x1, matrix products, project(): jnp.einsum('spd,dc->spc', tok_rows, key_projection_weight, preferred_elem...  5.93 us
    dot_general x2, matrix products, weigh(): jnp.einsum('skgl,slke->skge', weights, value_heads, preferred_element_typ...  5.84 us
    dot_general x1, matrix products, project(): jnp.einsum('spd,hd->shp', tok_rows, forget_gate_weight, preferred_element...  5.77 us
    all_to_all x2, local copies, waits for them, and re-layouts, local(): lax.all_to_all(rows_local, 'sp', split_axis=0, concat_axis=1, tiled=True)  5.47 us
  transfers between devices with their start and end apart: 2, of which 0 were waited for; matrix products, arithmetic and copies ran while one was open for 68% of the time, Pallas kernels for 0%

profile of v1, /device:TPU:0, one launch (start us, length us, event | category | flops | bytes accessed | tf_op | source)
XLA Modules:
  0.0 122.2 jit_solution(6102530760806221383)
XLA Ops:
  0.6 5.8 %fusion.20 = f32[8,4,256]{2,1,0:T(4,128)S(1)} fusion(f32[8,4,256]{2,1,0:T(4,128)} %param.21, f32[8,4,256]{2,1,0:T(4,128)} %param.20, bf16[8,256,2048]{2,1,0:T(8,128)(2,1)} %param.15, bf16[4,2048]{1,0:T(4,128)(2,1)} %param.18, f32[4]{0:T(128)} %param.19), kind=kOutput, calls=%fused_computation.31 | convolution fusion | flops 33644544 | bytes 8503312 | tf_op jit(solution)/shard_map/spd,hd->shp/dot_general | solution.py:33
  6.4 0.6 constant_dynamic-update-slice_fusion.7
  7.0 0.6 constant_dynamic-update-slice_fusion.6
  7.6 0.6 constant_dynamic-update-slice_fusion.5
  8.8 0.6 constant_dynamic-update-slice_fusion.3
  9.4 0.6 constant_dynamic-update-slice_fusion.2
  10.0 0.6 constant_dynamic-update-slice_fusion.1
  10.6 0.6 constant_dynamic-update-slice_fusion
  11.2 7.3 %all-to-all-start.1 = ((f32[8,1,4,256]{3,2,1,0:T(4,128)}), f32[8,1,4,256]{3,2,1,0:T(4,128)S(1)}, u32[]{:S(2)}, u32[]{:S(2)}) async-start(f32[8,1,4,256]{3,2,1,0:T(4,128)} %constant_dynamic-update-slice_fusion), calls=%async_computation.1 | async-start | bytes 65536 | tf_op jit(solution)/shard_map/all_to_all | solution.py:98
  18.5 5.9 %multiply_reduce_fusion = (f32[8,256,4]{1,2,0:T(4,128)S(1)}, f32[8,256,256]{1,2,0:T(8,128)S(1)}) fusion(bf16[8,256,2048]{2,1,0:T(8,128)(2,1)} %param.15, bf16[2048,256]{1,0:T(8,128)(2,1)S(1)} %copy-done), kind=kOutput, calls=%fused_computation.11 | convolution fusion | flops 2148524032 | bytes 11567104 | tf_op jit(solution)/shard_map/spd,dc->spc/dot_general | solution.py:18
  24.5 2.4 %convolution_convert_fusion = bf16[8,256,256]{1,2,0:T(8,128)(2,1)S(1)} fusion(bf16[8,256,2048]{2,1,0:T(8,128)(2,1)S(1)} %copy-done.2, bf16[2048,256]{1,0:T(8,128)(2,1)S(1)} %copy-done.9), kind=kOutput, calls=%fused_computation.12 | convolution fusion | flops 2148007936 | bytes 10485760 | tf_op jit(solution)/shard_map/spd,dc->spc/dot_general | solution.py:28
  27.5 1.5 %pad_maximum_fusion = bf16[8,256,4,128]{1,3,2,0:T(8,128)(2,1)} fusion(bf16[8,256,4,64]{1,3,2,0:T(8,128)(2,1)S(1)} %bitcast.110, bf16[8,256,4,64]{1,3,2,0:T(8,128)(2,1)S(1)} %multiply_convert_fusion), kind=kLoop, calls=%fused_computation.9 | loop fusion | flops 4194304 | bytes 4194304 | tf_op jit(solution)/shard_map/concatenate | solution.py:32
  29.0 6.0 %all-to-all-start = ((bf16[8,256,4,128]{1,3,2,0:T(8,128)(2,1)}), bf16[8,256,4,128]{1,3,2,0:T(8,128)(2,1)S(1)}, u32[]{:S(2)}, u32[]{:S(2)}) async-start(bf16[8,256,4,128]{1,3,2,0:T(8,128)(2,1)} %pad_maximum_fusion), calls=%async_computation | async-start | bytes 4194304 | tf_op jit(solution)/shard_map/all_to_all | solution.py:96
  35.0 20.9 %fusion.26 = (bf16[1,14336,4,64]{3,2,1,0:T(4,128)(2,1)}, bf16[1,14336,4,64]{3,2,1,0:T(4,128)(2,1)}) fusion(bf16[1,14336,4,128]{3,2,1,0:T(4,128)(2,1)} %param.22), kind=kLoop, calls=%fused_computation.72 | loop fusion | bytes 29360128 | tf_op jit(solution)/shard_map/slice | solution.py:49
  55.9 0.7 dynamic-slice_reduce_fusion
  56.7 21.4 %copy.37 = bf16[1,14336,4,64]{1,3,2,0:T(8,128)(2,1)} copy(bf16[1,14336,4,64]{3,2,1,0:T(4,128)(2,1)} %get-tuple-element.9) | data formatting | bytes 14680064
  78.3 21.4 %copy.38 = bf16[1,14336,4,64]{1,3,2,0:T(8,128)(2,1)} copy(bf16[1,14336,4,64]{3,2,1,0:T(4,128)(2,1)} %get-tuple-element.10) | data formatting | bytes 14680064
  100.2 1.2 reduce-window.6
  102.2 4.9 %fusion.27 = (f32[4,2]{1,0:T(4,128)S(1)}, f32[4,2,14336]{2,1,0:T(2,128)}) fusion(f32[4,14336]{1,0:T(4,128)S(1)} %bitcast.109, f32[4]{0:T(128)S(1)} %fusion.25, bf16[4,2,64]{2,1,0:T(2,128)(2,1)S(1)} %reshape.265, bf16[1,14336,4,64]{1,3,2,0:T(8,128)(2,1)} %copy.37), kind=kOutput, calls=%fused_computation.73 | convolution fusion | flops 15138808 | bytes 8029232 | tf_op jit(solution)/shard_map/skge,slke->skgl/dot_general | solution.py:50
  107.2 2.5 %copy.26 = bf16[8,256,4,128]{1,0,3,2:T(8,128)(2,1)} copy(bf16[8,256,4,128]{1,3,2,0:T(8,128)(2,1)S(1)} %all-to-all-done) | data formatting | bytes 4194304 | tf_op jit(solution)/shard_map/all_to_all | solution.py:96
  109.7 3.0 %all_to_all.13 = bf16[1,2048,4,128]{1,3,2,0:T(8,128)(2,1)S(1)} reshape(bf16[8,256,4,128]{1,0,3,2:T(8,128)(2,1)} %copy.26) | data formatting | bytes 4194304 | tf_op jit(solution)/shard_map/all_to_all | solution.py:96
  112.7 2.5 %copy.30 = bf16[1,2048,4,128]{3,2,1,0:T(4,128)(2,1)} copy(bf16[1,2048,4,128]{1,3,2,0:T(8,128)(2,1)S(1)} %all_to_all.13) | data formatting | bytes 4194304
  115.6 5.3 %fusion.11 = f32[4,2,64]{2,1,0:T(2,128)S(1)} fusion(bf16[1,14336,4,64]{1,3,2,0:T(8,128)(2,1)} %copy.38, f32[4,2,14336]{2,1,0:T(2,128)} %get-tuple-element.17, f32[4,2]{1,0:T(4,128)S(1)} %get-tuple-element.16, f32[4,2]{1,0:T(4,128)S(1)} %get-tuple-element.13), kind=kOutput, calls=%fused_computation.19 | convolution fusion | flops 14909952 | bytes 7800896 | tf_op jit(solution)/shard_map/skgl,slke->skge/dot_general | solution.py:61
  121.6 0.6 convert_element_type.52
  (54 shorter events, 3.8 us)
Async XLA Ops:
  0.6 17.9 %copy-start = (bf16[2048,256]{1,0:T(8,128)(2,1)S(1)}, bf16[2048,256]{1,0:T(8,128)(2,1)}, u32[]{:S(2)}) copy-start(bf16[2048,256]{1,0:T(8,128)(2,1)} %param.16) | copy-start | bytes 3145732
  11.2 17.8 %all-to-all-start.1 = ((f32[8,1,4,256]{3,2,1,0:T(4,128)}), f32[8,1,4,256]{3,2,1,0:T(4,128)S(1)}, u32[]{:S(2)}, u32[]{:S(2)}) async-start(f32[8,1,4,256]{3,2,1,0:T(4,128)} %constant_dynamic-update-slice_fusion), calls=%async_computation.1 | async-start | bytes 65536 | tf_op jit(solution)/shard_map/all_to_all | solution.py:98
  18.5 6.0 %copy-start.2 = (bf16[8,256,2048]{2,1,0:T(8,128)(2,1)S(1)}, bf16[8,256,2048]{2,1,0:T(8,128)(2,1)}, u32[]{:S(2)}) copy-start(bf16[8,256,2048]{2,1,0:T(8,128)(2,1)} %param.15) | copy-start | bytes 25165828
  18.5 6.0 %copy-start.9 = (bf16[2048,256]{1,0:T(8,128)(2,1)S(1)}, bf16[2048,256]{1,0:T(8,128)(2,1)}, u32[]{:S(2)}) copy-start(bf16[2048,256]{1,0:T(8,128)(2,1)} %param.17) | copy-start | bytes 3145732
  24.5 2.4 %copy-start.8 = (f32[64]{0:T(128)S(1)}, f32[64]{0:T(128)}, u32[]{:S(2)}) copy-start(f32[64]{0:T(128)} %param.28) | copy-start | bytes 772
  29.0 78.2 %all-to-all-start = ((bf16[8,256,4,128]{1,3,2,0:T(8,128)(2,1)}), bf16[8,256,4,128]{1,3,2,0:T(8,128)(2,1)S(1)}, u32[]{:S(2)}, u32[]{:S(2)}) async-start(bf16[8,256,4,128]{1,3,2,0:T(8,128)(2,1)} %pad_maximum_fusion), calls=%async_computation | async-start | bytes 4194304 | tf_op jit(solution)/shard_map/all_to_all | solution.py:96
  56.7 21.4 %copy-start.6 = (bf16[1,256]{1,0:T(2,128)(2,1)S(1)}, bf16[1,256]{1,0:T(2,128)(2,1)}, u32[]{:S(2)}) copy-start(bf16[1,256]{1,0:T(2,128)(2,1)} %param.25) | copy-start | bytes 1540
  78.3 21.5 %copy-start.7 = (bf16[1,256]{1,0:T(2,128)(2,1)S(1)}, bf16[1,256]{1,0:T(2,128)(2,1)}, u32[]{:S(2)}) copy-start(bf16[1,256]{1,0:T(2,128)(2,1)} %param.26) | copy-start | bytes 1540
  78.3 21.6 %copy-start.3 = (f32[1,4,14336]{2,1,0:T(4,128)S(1)}, f32[1,4,14336]{2,1,0:T(4,128)}, u32[]{:S(2)}) copy-start(f32[1,4,14336]{2,1,0:T(4,128)} %param.23) | copy-start | bytes 688132
  78.3 23.8 %copy-start.10 = (f32[1,4]{1,0:T(1,128)S(1)}, f32[1,4]{1,0:T(1,128)}, u32[]{:S(2)}) copy-start(f32[1,4]{1,0:T(1,128)} %param.27) | copy-start | bytes 52
  101.9 10.8 %copy-start.4 = (f32[1,4,2048]{2,1,0:T(4,128)}, f32[1,4,2048]{2,1,0:T(4,128)S(1)}, u32[]{:S(2)}) copy-start(f32[1,4,2048]{2,1,0:T(4,128)S(1)} %add_add_fusion) | copy-start | bytes 98308
  109.7 12.5 %copy-start.1 = (bf16[2048,256]{1,0:T(8,128)(2,1)S(1)}, bf16[2048,256]{1,0:T(8,128)(2,1)}, u32[]{:S(2)}) copy-start(bf16[2048,256]{1,0:T(8,128)(2,1)} %param.16) | copy-start | bytes 3145732
  112.6 8.9 %copy-start.5 = (f32[512]{0:T(512)S(1)}, f32[512]{0:T(512)}, u32[]{:S(2)}) copy-start(f32[512]{0:T(512)} %param.29) | copy-start | bytes 6148
